TPU v7x, 32 devices: a whole 2x2x4 slice. The times are simulated.
32 devices in a mesh: rep: 2 (over x), fs: 8 (over z, y), tp: 2 (over core).
Axes of the slice: x: 2, y: 2, z: 4, core: 2. Of those that a mesh axis runs over, the one named last changes fastest.
Arguments:
- tokens: bfloat16 [8192, 2048], P(('rep', 'fs', 'tp')), may hold values from -6 to 6
- norm_gain: float32 [2048], replicated, may hold values from 0.1 to 1.9
- gate_weight: float32 [2048, 5120], P('fs', 'tp'), may hold values from -0.125 to 0.125
- gate_scale: float32 [5120], P('tp'), may hold values from 0.1 to 1.9
- up_weight: float32 [2048, 5120], P('fs', 'tp'), may hold values from -0.125 to 0.125
- up_scale: float32 [5120], P('tp'), may hold values from 0.1 to 1.9
- down_weight: float32 [5120, 2048], P('tp', 'fs'), may hold values from -0.078125 to 0.078125
- down_scale: float32 [2048], replicated, may hold values from 0.1 to 1.9
Outputs:
- mixed: bfloat16 [8192, 2048], P(('rep', 'fs', 'tp'))
All inputs are finite; a program needn't handle non-finite values.
Results may differ from a plain program's by a relative error of at most 0.013.
Values may be sent and summed in bfloat16 or wider, within the bound.
A program may use at most 128 MiB of HBM per device.

v0:
```python
import jax
import jax.numpy as jnp
from jax import lax
from jax.sharding import PartitionSpec as P

EPS_VALUE = 1e-06


def from_partner(shard, axis, distance):
    return lax.ppermute(shard, axis, [(i, i ^ 1 << distance) for i in range(lax.axis_size(axis))])


def normalize(token_rows, norm_gain):
    values = token_rows.astype(jnp.float32)
    inverse = lax.rsqrt(jnp.mean(values * values, axis=-1, keepdims=True) + EPS_VALUE)
    return (values * inverse * norm_gain).astype(jnp.bfloat16)


def body(tokens, norm_gain, gate_weight, gate_scale, up_weight, up_scale, down_weight, down_scale):
    normed = normalize(tokens, norm_gain)
    gate_bf = gate_weight.astype(jnp.bfloat16)
    up_bf = up_weight.astype(jnp.bfloat16)
    down_bf = down_weight.astype(jnp.bfloat16)
    rep_index = lax.axis_index("rep")
    half_cols = gate_bf.shape[1] // 2
    half_rows = down_bf.shape[0] // 2
    own_gate = lax.dynamic_slice_in_dim(gate_bf, rep_index * half_cols, half_cols, 1)
    own_up = lax.dynamic_slice_in_dim(up_bf, rep_index * half_cols, half_cols, 1)
    own_down = lax.dynamic_slice_in_dim(down_bf, rep_index * half_rows, half_rows, 0)
    own_parts = (
        lax.all_gather(own_gate, "fs", axis=0, tiled=True),
        lax.all_gather(own_up, "fs", axis=0, tiled=True),
        lax.all_gather(own_down, "fs", axis=1, tiled=True),
    )
    far_parts = from_partner((own_parts[0], own_parts[1], own_parts[2]), "rep", 0)
    is_first = rep_index == 0

    def joined(own_part, far_part, axis_dim):
        return jnp.where(
            is_first,
            jnp.concatenate([own_part, far_part], axis_dim),
            jnp.concatenate([far_part, own_part], axis_dim),
        )

    gate_full = joined(own_parts[0], far_parts[0], 1)
    up_full = joined(own_parts[1], far_parts[1], 1)
    down_full = joined(own_parts[2], far_parts[2], 0)
    slab_rows = lax.all_gather(normed, "tp", axis=0, tiled=True)
    gate_pre = jnp.dot(slab_rows, gate_full, preferred_element_type=jnp.float32) * gate_scale
    up_pre = jnp.dot(slab_rows, up_full, preferred_element_type=jnp.float32) * up_scale
    hidden = (jax.nn.silu(gate_pre) * up_pre).astype(jnp.bfloat16)
    partial_value = (
        jnp.dot(hidden, down_full, preferred_element_type=jnp.float32) * down_scale
    ).astype(jnp.bfloat16)
    partial_value = lax.optimization_barrier(partial_value)
    return lax.psum_scatter(
        partial_value.astype(jnp.float32).astype(jnp.bfloat16),
        "tp",
        scatter_dimension=0,
        tiled=True,
    )


def solution(mesh):
    return jax.shard_map(
        body,
        mesh=mesh,
        in_specs=(
            P(("rep", "fs", "tp"), None),
            P(),
            P("fs", "tp"),
            P("tp"),
            P("fs", "tp"),
            P("tp"),
            P("tp", "fs"),
            P(),
        ),
        out_specs=P(("rep", "fs", "tp"), None),
        check_vma=False,
    )
```

profile of v0, /device:TPU:0, one launch (start us, length us, event | category | flops | bytes accessed | tf_op | source)
XLA Modules:
  0.0 482.2 jit_solution(2602292842199333268)
XLA Ops:
  7.4 0.0 copy-start
  7.4 0.0 copy-start.1
  7.4 0.0 all-gather.7.cloned.1.call-start
  7.4 1.7 copy-done
  9.1 0.9 dynamic-slice_convert_fusion.2
  10.0 0.0 all-gather.7.cloned.1.call-update
  10.1 0.0 all-gather.9.cloned.1.call-start
  10.1 2.2 dynamic-slice_convert_fusion.1
  12.3 0.0 all-gather.9.cloned.1.call-update
  12.4 0.0 all-gather.11.cloned.1.call-start
  12.4 2.2 dynamic-slice_convert_fusion
  14.6 0.0 all-gather.11.cloned.1.call-update
  14.7 0.0 all-gather.5.cloned.1.call-start
  14.7 84.3 %all-gather.7.cloned.1.call-done = bf16[2048,1280]{1,0:T(8,128)(2,1)} async-done(((bf16[256,1280]{1,0:T(8,128)(2,1)}), bf16[2048,1280]{1,0:T(8,128)(2,1)}) %all-gather.7.cloned.1.call-update) | async-done | bytes 5242896 | tf_op jit(solution)/shard_map/all_gather | solution.py:31
  99.0 1.5 collective-permute-start
  100.5 84.8 %all-gather.9.cloned.1.call-done = bf16[2048,1280]{1,0:T(8,128)(2,1)} async-done(((bf16[256,1280]{1,0:T(8,128)(2,1)}), bf16[2048,1280]{1,0:T(8,128)(2,1)}) %all-gather.9.cloned.1.call-update) | async-done | bytes 5242896 | tf_op jit(solution)/shard_map/all_gather | solution.py:32
  185.3 1.5 collective-permute-start.1
  186.7 85.6 %all-gather.11.cloned.1.call-done = bf16[1280,2048]{1,0:T(8,128)(2,1)} async-done(((bf16[1280,256]{1,0:T(8,128)(2,1)}), bf16[1280,2048]{1,0:T(8,128)(2,1)}) %all-gather.11.cloned.1.call-update) | async-done | bytes 5242896 | tf_op jit(solution)/shard_map/all_gather | solution.py:33
  272.3 1.5 collective-permute-start.2
  273.8 1.5 fusion.21
  275.3 0.0 copy-done.1
  275.4 2.5 fusion.23
  277.9 0.0 all-gather.5.cloned.1.call-update
  277.9 0.0 reduce-scatter.2.cloned.1.call-start
  277.9 0.0 copy-start.2
  278.0 0.0 copy-start.3
  278.0 0.0 copy-start.4
  278.0 7.7 %all-gather.5.cloned.1.call-done = bf16[512,2048]{1,0:T(8,128)(2,1)} async-done(((bf16[256,2048]{1,0:T(8,128)(2,1)}), bf16[512,2048]{1,0:T(8,128)(2,1)}) %all-gather.5.cloned.1.call-update) | async-done | bytes 2097168 | tf_op jit(solution)/shard_map/all_gather | solution.py:48
  285.7 0.0 collective-permute-done
  285.7 15.7 %fusion = f32[512,2560]{1,0:T(8,128)} fusion(bf16[512,2048]{1,0:T(8,128)(2,1)} %all-gather.5.cloned.1.call-done, bf16[2048,1280]{1,0:T(8,128)(2,1)} %collective-permute-done, bf16[2048,1280]{1,0:T(8,128)(2,1)} %all-gather.7.cloned.1.call-done, pred[]{:T(512)S(6)} %eq.3), kind=kOutput, calls=%fused_computation.1 | convolution fusion | flops 5415895040 | bytes 17825792 | tf_op jit(solution)/shard_map/dot_general | solution.py:49
  301.4 26.2 %collective-permute-done.1 = bf16[2048,1280]{1,0:T(8,128)(2,1)} collective-permute-done((bf16[2048,1280]{1,0:T(8,128)(2,1)}, bf16[2048,1280]{1,0:T(8,128)(2,1)}, u32[]{:S(2)}, u32[]{:S(2)}) %collective-permute-start.1) | collective-permute-done | bytes 5242912 | tf_op jit(solution)/shard_map/ppermute | solution.py:10
  327.6 109.7 %collective-permute-done.2 = bf16[1280,2048]{1,0:T(8,128)(2,1)} collective-permute-done((bf16[1280,2048]{1,0:T(8,128)(2,1)}, bf16[1280,2048]{1,0:T(8,128)(2,1)}, u32[]{:S(2)}, u32[]{:S(2)}) %collective-permute-start.2) | collective-permute-done | bytes 5242912 | tf_op jit(solution)/shard_map/ppermute | solution.py:10
  437.2 0.0 copy-done.2
  437.2 0.0 copy-done.3
  437.2 0.0 copy-done.4
  437.2 28.2 %multiply_convert_fusion.1 = bf16[512,2048]{1,0:T(8,128)(2,1)} fusion(bf16[1280,2048]{1,0:T(8,128)(2,1)} %collective-permute-done.2, bf16[1280,2048]{1,0:T(8,128)(2,1)} %all-gather.11.cloned.1.call-done, pred[]{:T(512)S(6)} %eq.3, f32[2048]{0:T(1024)S(1)} %copy-done.4, f32[512,2560]{1,0:T(8,128)} %fusion, ...), kind=kOutput, calls=%fused_computation.25 | convolution fusion | flops 10844372992 | bytes 30437376 | tf_op jit(solution)/shard_map/dot_general | solution.py:53
  465.5 0.0 reduce-scatter.2.cloned.1.call-update
  465.5 9.5 %reduce-scatter.2.cloned.1.call-done = bf16[256,2048]{1,0:T(8,128)(2,1)} async-done(((bf16[512,2048]{1,0:T(8,128)(2,1)}), bf16[256,2048]{1,0:T(8,128)(2,1)}) %reduce-scatter.2.cloned.1.call-update) | async-done | bytes 1048592 | tf_op jit(solution)/shard_map/reduce_scatter | solution.py:56
  (1 shorter events, 0.0 us)
Async XLA Ops:
  7.4 1.7 copy-start
  7.4 268.0 %copy-start.1 = (f32[2048]{0:T(1024)S(1)}, f32[2048]{0:T(1024)}, u32[]{:S(2)}) copy-start(f32[2048]{0:T(1024)} %param.9) | copy-start | bytes 24580
  7.4 91.6 %all-gather.7.cloned.1.call-start = ((), (), s32[]{:S(2)}) async-start(), calls=%async_computation.2 | async-start | bytes 5898240 | tf_op jit(solution)/shard_map/all_gather | solution.py:31
  10.1 175.2 %all-gather.9.cloned.1.call-start = ((), (), s32[]{:S(2)}) async-start(), calls=%async_computation.3 | async-start | bytes 5898240 | tf_op jit(solution)/shard_map/all_gather | solution.py:32
  12.4 259.9 %all-gather.11.cloned.1.call-start = ((), (), s32[]{:S(2)}) async-start(), calls=%async_computation.4 | async-start | bytes 5898240 | tf_op jit(solution)/shard_map/all_gather | solution.py:33
  14.7 271.0 %all-gather.5.cloned.1.call-start = ((), (), s32[]{:S(2)}) async-start(), calls=%async_computation.1 | async-start | bytes 3145728 | tf_op jit(solution)/shard_map/all_gather | solution.py:48
  99.0 186.7 %collective-permute-start = (bf16[2048,1280]{1,0:T(8,128)(2,1)}, bf16[2048,1280]{1,0:T(8,128)(2,1)}, u32[]{:S(2)}, u32[]{:S(2)}) collective-permute-start(bf16[2048,1280]{1,0:T(8,128)(2,1)} %all-gather.7.cloned.1.call-done), channel_id=1, source_target_pairs={{0,16},{16,0},{1,17},{17,1},{2,18},{18,2},{3,19},{19,3},{4,20},{20... | collective-permute-start | bytes 15728648 | tf_op jit(solution)/shard_map/ppermute | solution.py:10
  185.3 142.3 %collective-permute-start.1 = (bf16[2048,1280]{1,0:T(8,128)(2,1)}, bf16[2048,1280]{1,0:T(8,128)(2,1)}, u32[]{:S(2)}, u32[]{:S(2)}) collective-permute-start(bf16[2048,1280]{1,0:T(8,128)(2,1)} %all-gather.9.cloned.1.call-done), channel_id=1, source_target_pairs={{0,16},{16,0},{1,17},{17,1},{2,18},{18,2},{3,19},{19,3},{4,20},{20... | collective-permute-start | bytes 15728648 | tf_op jit(solution)/shard_map/ppermute | solution.py:10
  272.3 164.9 %collective-permute-start.2 = (bf16[1280,2048]{1,0:T(8,128)(2,1)}, bf16[1280,2048]{1,0:T(8,128)(2,1)}, u32[]{:S(2)}, u32[]{:S(2)}) collective-permute-start(bf16[1280,2048]{1,0:T(8,128)(2,1)} %all-gather.11.cloned.1.call-done), channel_id=1, source_target_pairs={{0,16},{16,0},{1,17},{17,1},{2,18},{18,2},{3,19},{19,3},{4,20},{20... | collective-permute-start | bytes 15728648 | tf_op jit(solution)/shard_map/ppermute | solution.py:10
  277.9 197.2 %reduce-scatter.2.cloned.1.call-start = ((), (), s32[]{:S(2)}) async-start(), calls=%async_computation.5 | async-start | bytes 3145728 | tf_op jit(solution)/shard_map/reduce_scatter | solution.py:56
  277.9 159.3 %copy-start.2 = (f32[2560]{0:T(1024)S(1)}, f32[2560]{0:T(1024)}, u32[]{:S(2)}) copy-start(f32[2560]{0:T(1024)} %param.13) | copy-start | bytes 30724
  278.0 159.3 %copy-start.3 = (f32[2560]{0:T(1024)S(1)}, f32[2560]{0:T(1024)}, u32[]{:S(2)}) copy-start(f32[2560]{0:T(1024)} %param.11) | copy-start | bytes 30724
  278.0 159.3 %copy-start.4 = (f32[2048]{0:T(1024)S(1)}, f32[2048]{0:T(1024)}, u32[]{:S(2)}) copy-start(f32[2048]{0:T(1024)} %param.15) | copy-start | bytes 24580
Sparse Core Ops, SparseCore 0:
  10.4 88.5 all-gather.6
  101.2 84.0 all-gather.8
  187.3 84.9 all-gather.10
Sparse Core Ops, SparseCore 1:
  278.0 7.7 all-gather.4
  465.6 9.4 reduce-scatter.1
where the time goes:
time: 482 us
  waiting for transfers between devices  408 us (85%)
  matrix products  43.9 us (9%)
  between operations  14.6 us (3%)
  local copies, waits for them, and re-layouts  7.14 us (1%)
    ppermute x3, waiting for transfers between devices, from_partner(): lax.ppermute(shard, axis, [(i, i ^ 1 << distance) for i in range(lax.axis...  136 us
    all_gather x1, waiting for transfers between devices, body(): lax.all_gather(own_down, 'fs', axis=1, tiled=True)  85.6 us
    all_gather x1, waiting for transfers between devices, body(): lax.all_gather(own_up, 'fs', axis=0, tiled=True)  84.8 us
    all_gather x1, waiting for transfers between devices, body(): lax.all_gather(own_gate, 'fs', axis=0, tiled=True)  84.3 us
    dot_general x1, matrix products, body(): jnp.dot(hidden, down_full, preferred_element_type=jnp.float32) * down_scale  28.2 us
    dot_general x1, matrix products, body(): jnp.dot(slab_rows, gate_full, preferred_element_type=jnp.float32)  15.7 us
  transfers between devices with their start and end apart: 8, of which 7 were waited for; matrix products, arithmetic and copies ran while one was open for 5% of the time, Pallas kernels for 0%

commit v1 on v0

--- a/solution.py
+++ b/solution.py
@@ -30,7 +30,7 @@
     own_parts = (
         lax.all_gather(own_gate, "fs", axis=0, tiled=True),
         lax.all_gather(own_up, "fs", axis=0, tiled=True),
-        lax.all_gather(own_down, "fs", axis=1, tiled=True),
+        jnp.concatenate(lax.all_gather(own_down, "fs"), axis=1),
     )
     far_parts = from_partner((own_parts[0], own_parts[1], own_parts[2]), "rep", 0)
     is_first = rep_index == 0

time: 482 us -> 482 us (level)
  waiting for transfers between devices: 408 us -> 400 us
  local copies, waits for them, and re-layouts: 7.14 us -> 15 us
    reshape x0 -> x1, local copies, waits for them, and re-layouts: none -> 7.88 us  [body(): jnp.concatenate(lax.all_gather(own_down, 'fs'), axis=1)]
    all_gather x1, waiting for transfers between devices: 84.8 us -> 76.9 us  [body(): lax.all_gather(own_up, 'fs', axis=0, tiled=True)]
  transfers between devices with their start and end apart: 8 -> 8, of which waited for: 7 -> 7; matrix products, arithmetic and copies ran while one was open for 5% -> 7% of each run, Pallas kernels for 0% -> 0%
where the time goes in v1:
time: 482 us; the launch traced here: 481 us
  waiting for transfers between devices  400 us (83%)
  matrix products  42.9 us (9%)
  local copies, waits for them, and re-layouts  15 us (3%)
  between operations  14.6 us (3%)
    ppermute x3, waiting for transfers between devices, from_partner(): lax.ppermute(shard, axis, [(i, i ^ 1 << distance) for i in range(lax.axis...  137 us
    all_gather x1, waiting for transfers between devices, body(): lax.all_gather(own_down, 'fs')  84.8 us
    all_gather x1, waiting for transfers between devices, body(): lax.all_gather(own_gate, 'fs', axis=0, tiled=True)  84.3 us
    all_gather x1, waiting for transfers between devices, body(): lax.all_gather(own_up, 'fs', axis=0, tiled=True)  76.9 us
    dot_general x1, matrix products, body(): jnp.dot(hidden, down_full, preferred_element_type=jnp.float32) * down_scale  27.5 us
    dot_general x1, matrix products, body(): jnp.dot(slab_rows, gate_full, preferred_element_type=jnp.float32)  15.4 us
  transfers between devices with their start and end apart: 8, of which 7 were waited for; matrix products, arithmetic and copies ran while one was open for 7% of the time, Pallas kernels for 0%

profile of v1, /device:TPU:0, one launch (start us, length us, event | category | flops | bytes accessed | tf_op | source)
XLA Modules:
  0.0 481.5 jit_solution(4549564527161563936)
XLA Ops:
  7.4 0.0 copy-start
  7.4 0.0 all-gather.8.cloned.1.call-start
  7.4 1.7 copy-done
  9.1 0.9 dynamic-slice_convert_fusion.2
  10.0 0.0 all-gather.8.cloned.1.call-update
  10.0 0.0 all-gather.12.cloned.1.call-start
  10.1 2.2 dynamic-slice_convert_fusion
  12.3 0.0 all-gather.12.cloned.1.call-update
  12.3 0.0 all-gather.10.cloned.1.call-start
  12.4 2.2 dynamic-slice_convert_fusion.1
  14.6 0.0 all-gather.10.cloned.1.call-update
  14.6 0.0 all-gather.6.cloned.1.call-start
  14.7 84.3 %all-gather.8.cloned.1.call-done = bf16[2048,1280]{1,0:T(8,128)(2,1)} async-done(((bf16[256,1280]{1,0:T(8,128)(2,1)}), bf16[2048,1280]{1,0:T(8,128)(2,1)}) %all-gather.8.cloned.1.call-update) | async-done | bytes 5242896 | tf_op jit(solution)/shard_map/all_gather | solution.py:31
  99.0 1.5 collective-permute-start
  100.5 84.8 %all-gather.12.cloned.1.call-done = bf16[10240,256]{1,0:T(8,128)(2,1)} async-done(((bf16[1280,256]{1,0:T(8,128)(2,1)}), bf16[10240,256]{1,0:T(8,128)(2,1)}) %all-gather.12.cloned.1.call-update) | async-done | bytes 5242896 | tf_op jit(solution)/shard_map/all_gather | solution.py:33
  185.3 0.0 copy-start.1
  185.3 7.9 %copy.9 = bf16[1280,8,256]{0,2,1:T(8,128)(2,1)} copy(bf16[1280,8,256]{2,0,1:T(8,128)(2,1)} %bitcast.8) | data formatting | bytes 10485760 | tf_op jit(solution)/shard_map/reshape | solution.py:33
  193.1 1.5 collective-permute-start.2
  194.6 76.9 %all-gather.10.cloned.1.call-done = bf16[2048,1280]{1,0:T(8,128)(2,1)} async-done(((bf16[256,1280]{1,0:T(8,128)(2,1)}), bf16[2048,1280]{1,0:T(8,128)(2,1)}) %all-gather.10.cloned.1.call-update) | async-done | bytes 5242896 | tf_op jit(solution)/shard_map/all_gather | solution.py:32
  271.6 1.5 collective-permute-start.1
  273.0 1.5 fusion.21
  274.5 0.0 copy-done.1
  274.6 2.5 fusion.23
  277.1 0.0 all-gather.6.cloned.1.call-update
  277.1 0.0 reduce-scatter.2.cloned.1.call-start
  277.1 0.0 copy-start.2
  277.2 0.0 copy-start.3
  277.2 0.0 copy-start.4
  277.2 7.8 %all-gather.6.cloned.1.call-done = bf16[512,2048]{1,0:T(8,128)(2,1)} async-done(((bf16[256,2048]{1,0:T(8,128)(2,1)}), bf16[512,2048]{1,0:T(8,128)(2,1)}) %all-gather.6.cloned.1.call-update) | async-done | bytes 2097168 | tf_op jit(solution)/shard_map/all_gather | solution.py:48
  284.9 0.0 collective-permute-done
  284.9 15.4 %fusion = f32[512,2560]{1,0:T(8,128)} fusion(bf16[512,2048]{1,0:T(8,128)(2,1)} %all-gather.6.cloned.1.call-done, bf16[2048,1280]{1,0:T(8,128)(2,1)} %collective-permute-done, bf16[2048,1280]{1,0:T(8,128)(2,1)} %all-gather.8.cloned.1.call-done, pred[]{:T(512)S(6)} %eq.3), kind=kOutput, calls=%fused_computation.1 | convolution fusion | flops 5415895040 | bytes 17825792 | tf_op jit(solution)/shard_map/dot_general | solution.py:49
  300.3 27.3 %collective-permute-done.2 = bf16[1280,2048]{0,1:T(8,128)(2,1)} collective-permute-done((bf16[1280,2048]{0,1:T(8,128)(2,1)}, bf16[1280,2048]{0,1:T(8,128)(2,1)}, u32[]{:S(2)}, u32[]{:S(2)}) %collective-permute-start.2) | collective-permute-done | bytes 5242912 | tf_op jit(solution)/shard_map/ppermute | solution.py:10
  327.6 109.7 %collective-permute-done.1 = bf16[2048,1280]{1,0:T(8,128)(2,1)} collective-permute-done((bf16[2048,1280]{1,0:T(8,128)(2,1)}, bf16[2048,1280]{1,0:T(8,128)(2,1)}, u32[]{:S(2)}, u32[]{:S(2)}) %collective-permute-start.1) | collective-permute-done | bytes 5242912 | tf_op jit(solution)/shard_map/ppermute | solution.py:10
  437.2 0.0 copy-done.2
  437.2 0.0 copy-done.3
  437.2 0.0 copy-done.4
  437.2 27.5 %multiply_convert_fusion.1 = bf16[512,2048]{1,0:T(8,128)(2,1)} fusion(bf16[1280,2048]{0,1:T(8,128)(2,1)} %collective-permute-done.2, bf16[1280,2048]{0,1:T(8,128)(2,1)} %bitcast.7, pred[]{:T(512)S(6)} %eq.3, f32[2048]{0:T(1024)S(1)} %copy-done.4, f32[512,2560]{1,0:T(8,128)} %fusion, bf16[512,2048]{1,0:T(8,128)(2,1)} %all-gather.6.cloned.1.call-done, ...), kind=kOutput, calls=%fused_computation.25 | convolution fusion | flops 10844372992 | bytes 30437376 | tf_op jit(solution)/shard_map/dot_general | solution.py:53
  464.8 0.0 reduce-scatter.2.cloned.1.call-update
  464.8 9.5 %reduce-scatter.2.cloned.1.call-done = bf16[256,2048]{1,0:T(8,128)(2,1)} async-done(((bf16[512,2048]{1,0:T(8,128)(2,1)}), bf16[256,2048]{1,0:T(8,128)(2,1)}) %reduce-scatter.2.cloned.1.call-update) | async-done | bytes 1048592 | tf_op jit(solution)/shard_map/reduce_scatter | solution.py:56
  (1 shorter events, 0.0 us)
Async XLA Ops:
  7.4 1.7 copy-start
  7.4 91.6 %all-gather.8.cloned.1.call-start = ((), (), s32[]{:S(2)}) async-start(), calls=%async_computation.2 | async-start | bytes 5898240 | tf_op jit(solution)/shard_map/all_gather | solution.py:31
  10.0 175.2 %all-gather.12.cloned.1.call-start = ((), (), s32[]{:S(2)}) async-start(), calls=%async_computation.5 | async-start | bytes 5898240 | tf_op jit(solution)/shard_map/all_gather | solution.py:33
  12.3 259.2 %all-gather.10.cloned.1.call-start = ((), (), s32[]{:S(2)}) async-start(), calls=%async_computation.3 | async-start | bytes 5898240 | tf_op jit(solution)/shard_map/all_gather | solution.py:32
  14.6 270.3 %all-gather.6.cloned.1.call-start = ((), (), s32[]{:S(2)}) async-start(), calls=%async_computation.1 | async-start | bytes 3145728 | tf_op jit(solution)/shard_map/all_gather | solution.py:48
  99.0 185.9 %collective-permute-start = (bf16[2048,1280]{1,0:T(8,128)(2,1)}, bf16[2048,1280]{1,0:T(8,128)(2,1)}, u32[]{:S(2)}, u32[]{:S(2)}) collective-permute-start(bf16[2048,1280]{1,0:T(8,128)(2,1)} %all-gather.8.cloned.1.call-done), channel_id=1, source_target_pairs={{0,16},{16,0},{1,17},{17,1},{2,18},{18,2},{3,19},{19,3},{4,20},{20... | collective-permute-start | bytes 15728648 | tf_op jit(solution)/shard_map/ppermute | solution.py:10
  185.3 89.3 %copy-start.1 = (f32[2048]{0:T(1024)S(1)}, f32[2048]{0:T(1024)}, u32[]{:S(2)}) copy-start(f32[2048]{0:T(1024)} %param.9) | copy-start | bytes 24580
  193.1 134.4 %collective-permute-start.2 = (bf16[1280,2048]{0,1:T(8,128)(2,1)}, bf16[1280,2048]{0,1:T(8,128)(2,1)}, u32[]{:S(2)}, u32[]{:S(2)}) collective-permute-start(bf16[1280,2048]{0,1:T(8,128)(2,1)} %bitcast.6), channel_id=1, source_target_pairs={{0,16},{16,0},{1,17},{17,1},{2,18},{18,2},{3,19},{19,3},{4,20},{20... | collective-permute-start | bytes 15728648 | tf_op jit(solution)/shard_map/ppermute | solution.py:10
  271.6 165.7 %collective-permute-start.1 = (bf16[2048,1280]{1,0:T(8,128)(2,1)}, bf16[2048,1280]{1,0:T(8,128)(2,1)}, u32[]{:S(2)}, u32[]{:S(2)}) collective-permute-start(bf16[2048,1280]{1,0:T(8,128)(2,1)} %all-gather.10.cloned.1.call-done), channel_id=1, source_target_pairs={{0,16},{16,0},{1,17},{17,1},{2,18},{18,2},{3,19},{19,3},{4,20},{20... | collective-permute-start | bytes 15728648 | tf_op jit(solution)/shard_map/ppermute | solution.py:10
  277.1 197.3 %reduce-scatter.2.cloned.1.call-start = ((), (), s32[]{:S(2)}) async-start(), calls=%async_computation.4 | async-start | bytes 3145728 | tf_op jit(solution)/shard_map/reduce_scatter | solution.py:56
  277.1 160.1 %copy-start.2 = (f32[2560]{0:T(1024)S(1)}, f32[2560]{0:T(1024)}, u32[]{:S(2)}) copy-start(f32[2560]{0:T(1024)} %param.13) | copy-start | bytes 30724
  277.2 160.1 %copy-start.3 = (f32[2560]{0:T(1024)S(1)}, f32[2560]{0:T(1024)}, u32[]{:S(2)}) copy-start(f32[2560]{0:T(1024)} %param.11) | copy-start | bytes 30724
  277.2 160.1 %copy-start.4 = (f32[2048]{0:T(1024)S(1)}, f32[2048]{0:T(1024)}, u32[]{:S(2)}) copy-start(f32[2048]{0:T(1024)} %param.15) | copy-start | bytes 24580
Sparse Core Ops, SparseCore 0:
  10.3 88.5 all-gather.7
  101.2 84.0 all-gather.11
  187.5 84.0 all-gather.9
Sparse Core Ops, SparseCore 1:
  277.2 7.7 all-gather.5
  464.9 9.4 reduce-scatter.1
